TPU v7x, 32 devices: a whole 2x2x4 slice. The times are simulated.
32 devices in a mesh: ra: 8 (over z, x), cb: 4 (over y, core).
Axes of the slice: x: 2, y: 2, z: 4, core: 2. Of those that a mesh axis runs over, the one named last changes fastest.
Arguments:
- tokens: bfloat16 [384, 4096], P(None, 'ra'), may hold values from -260 to 260
- up_weight: float32 [2, 4096, 16384], P(None, 'ra', 'cb'), may hold values from -0.125 to 0.125
- up_scale: float32 [2, 16384], P(None, 'cb'), may hold values from 0.5 to 2
- down_weight: float32 [2, 16384, 4096], P(None, 'cb', 'ra'), may hold values from -0.046875 to 0.046875
- down_scale: float32 [2, 4096], P(None, 'ra'), may hold values from 0.7 to 14
- pre_gain: float32 [2, 4096], P(None, 'ra'), may hold values from 0.1 to 1.9
- post_gain: float32 [2, 4096], P(None, 'ra'), may hold values from 0.1 to 1.9
Outputs:
- stream_out: bfloat16 [384, 4096], P(None, 'ra')
All inputs are finite; a program needn't handle non-finite values.
Results may differ from a plain program's by a relative error of at most 0.023.
Values may be sent and summed in bfloat16 or wider, within the bound.
A program may use at most 128 MiB of HBM per device.

v0:
```python
import functools

import jax
import jax.numpy as jnp
from jax import lax
from jax.experimental import pallas as pl
from jax.experimental.pallas import tpu as pltpu
from jax.sharding import PartitionSpec as P

norm_eps = 1e-06
residual_keep = 0.5
MESH = pl.DeviceIdType.MESH
FLOWS = 8
LANES = 128
BF16_ROWS = 16


def plain(tokens, up_weight, up_scale, down_weight, down_scale, pre_gain, post_gain):
    values = tokens.astype(jnp.float32)
    model_width = tokens.shape[1] * lax.axis_size("ra")
    stream = tokens
    for sublayer in range(up_weight.shape[0]):
        scaled = (values * pre_gain[sublayer][None, :]).astype(jnp.bfloat16)
        up_matrix = up_weight[sublayer].astype(jnp.bfloat16)
        down_matrix = down_weight[sublayer].astype(jnp.bfloat16)
        partial_up = jnp.dot(scaled, up_matrix, preferred_element_type=jnp.float32)
        whole_up = lax.psum(partial_up.astype(jnp.bfloat16), "ra").astype(jnp.float32)
        hidden = jnp.square(jax.nn.relu(whole_up * up_scale[sublayer][None, :])).astype(
            jnp.bfloat16
        )
        partial_down = jnp.dot(hidden, down_matrix, preferred_element_type=jnp.float32)
        summed = lax.psum(partial_down.astype(jnp.bfloat16), "cb").astype(jnp.float32)
        branch_in = summed * down_scale[sublayer][None, :]
        post_squares = lax.psum(jnp.sum(branch_in * branch_in, axis=1), "ra")
        inv_post = lax.rsqrt(post_squares / model_width + norm_eps)[:, None]
        branch = branch_in * inv_post * post_gain[sublayer][None, :]
        stream = (residual_keep * values + branch).astype(jnp.bfloat16)
        values = stream.astype(jnp.float32)
    return stream


def kernel(
    n, m, layers,
    tok, up, us, dn, ds, pg, qg,
    out,
    st_up, st_dn, wu, wd, xs, own, sendb, recvb, hid, accd, cbb, bbuf, ssq, ssall,
    w_sem, rs_s, rs_r, ag_s, ag_r, cb_s, cb_r, ss_s, ss_r,
):
    f32, bf16 = jnp.float32, jnp.bfloat16
    ra, cb = lax.axis_index("ra"), lax.axis_index("cb")
    rows, dl = tok.shape[1], tok.shape[2]
    fq = wu.shape[2]
    tokens = n * rows

    def wrap(i):
        return lax.rem(i + 2 * n, n)

    half, odd = lax.div(ra, 2), lax.rem(ra, 2)
    p = half + odd * (n - 1 - 2 * half)

    def ra_of(q):
        hi = lax.div(q, n // 2)
        return 2 * q * (1 - hi) + hi * (2 * (n - 1 - q) + 1)

    right, left = ra_of(wrap(p + 1)), ra_of(wrap(p - 1))
    order = [i + j for i in range(FLOWS // 2) for j in (0, FLOWS // 2)]
    sign = [1 if f < FLOWS // 2 else -1 for f in range(FLOWS)]
    target = [right if f < FLOWS // 2 else left for f in range(FLOWS)]

    def up_copy(l, f):
        return pltpu.make_async_copy(
            up.at[l, :, pl.ds(f * fq, fq)], st_up.at[f], w_sem.at[0, f]
        )

    def dn_copy(l, f):
        return pltpu.make_async_copy(
            dn.at[l, pl.ds(f * fq, fq), :], st_dn.at[f], w_sem.at[1, f]
        )

    def convert(src, dst, f, block):
        def body(i, _):
            r = pl.ds(pl.multiple_of(i * block, block), block)
            dst[f, r, :] = src[f, r, :].astype(bf16)
            return 0

        lax.fori_loop(0, src.shape[1] // block, body, 0)

    def convert_up(l):
        for f in order:
            up_copy(l, f).wait()
            convert(st_up, wu, f, min(64, dl))
        if l + 1 < layers:
            for f in order:
                up_copy(l + 1, f).start()

    def convert_dn(l):
        for f in order:
            dn_copy(l, f).wait()
            convert(st_dn, wd, f, min(128, fq))
        if l + 1 < layers:
            for f in order:
                dn_copy(l + 1, f).start()

    def rs_copy(l, f, s):
        return pltpu.make_async_remote_copy(
            src_ref=sendb.at[f, s], dst_ref=recvb.at[l, f, s],
            send_sem=rs_s.at[l, f, s], recv_sem=rs_r.at[l, f, s],
            device_id={"ra": target[f]}, device_id_type=MESH,
        )

    def ag_copy(l, f, s):
        c = wrap(p - sign[f] * (s - 1))
        return pltpu.make_async_remote_copy(
            src_ref=hid.at[l, c, f], dst_ref=hid.at[l, c, f],
            send_sem=ag_s.at[l, f, s - 1], recv_sem=ag_r.at[l, f, s - 1],
            device_id={"ra": target[f]}, device_id_type=MESH,
        )

    def ag_arrival(l, f, s):
        c = wrap(p - sign[f] * s)
        return pltpu.make_async_remote_copy(
            src_ref=hid.at[l, c, f], dst_ref=hid.at[l, c, f],
            send_sem=ag_s.at[l, f, s - 1], recv_sem=ag_r.at[l, f, s - 1],
            device_id={"ra": target[f]}, device_id_type=MESH,
        )

    def cb_copy(l, k, c, who):
        return pltpu.make_async_remote_copy(
            src_ref=cbb.at[l, who, c], dst_ref=cbb.at[l, who, c],
            send_sem=cb_s.at[l, k - 1, c], recv_sem=cb_r.at[l, k - 1, c],
            device_id={"cb": lax.rem(cb + k, m)}, device_id_type=MESH,
        )

    def ss_copy(l, k, who):
        return pltpu.make_async_remote_copy(
            src_ref=ssall.at[l, who], dst_ref=ssall.at[l, who],
            send_sem=ss_s.at[l, k - 1], recv_sem=ss_r.at[l, k - 1],
            device_id={"ra": lax.rem(ra + k, n)}, device_id_type=MESH,
        )

    def dot(a, b):
        return jnp.dot(a, b, preferred_element_type=f32)

    for f in order:
        up_copy(0, f).start()
    for f in order:
        dn_copy(0, f).start()

    barrier = pltpu.get_barrier_semaphore()
    for k in range(1, n):
        pl.semaphore_signal(
            barrier, inc=1, device_id={"ra": lax.rem(ra + k, n)}, device_id_type=MESH
        )
    for k in range(1, m):
        pl.semaphore_signal(
            barrier, inc=1, device_id={"cb": lax.rem(cb + k, m)}, device_id_type=MESH
        )

    def scale_in(c, _):
        xs[c] = (tok[c].astype(f32) * pg[0:1, :]).astype(bf16)
        return 0

    lax.fori_loop(0, n, scale_in, 0)
    pl.semaphore_wait(barrier, n + m - 2)

    for l in range(layers):
        if l == 0:
            for f in order:
                up_copy(l, f).wait()
                convert(st_up, wu, f, min(64, dl))
                sendb[f, 0] = dot(xs[wrap(p - sign[f])], wu[f]).astype(bf16)
                rs_copy(l, f, 0).start()
            for f in order:
                if layers > 1:
                    up_copy(l + 1, f).start()
        else:
            for f in order:
                sendb[f, 0] = dot(xs[wrap(p - sign[f])], wu[f]).astype(bf16)
                rs_copy(l, f, 0).start()
        convert_dn(l)

        def rs_step(s, _):
            for f in order:
                own[f] = dot(xs[wrap(p - sign[f] * (2 + s))], wu[f])
            for f in order:
                rs_copy(l, f, s).wait_recv()
                sendb[f, s + 1] = (recvb[l, f, s].astype(f32) + own[f]).astype(bf16)
                rs_copy(l, f, s + 1).start()
            return 0

        lax.fori_loop(0, n - 2, rs_step, 0)
        for f in order:
            own[f] = dot(xs[p], wu[f])
        for f in order:
            rs_copy(l, f, n - 2).wait_recv()
            v = recvb[l, f, n - 2].astype(f32) + own[f]
            v = jnp.maximum(v * us[l : l + 1, f * fq : (f + 1) * fq], 0.0)
            hid[l, p, f] = (v * v).astype(bf16)
            ag_copy(l, f, 1).start()

        def finish(c):
            cbb[l, cb, c] = accd[c].astype(bf16)
            for k in range(1, m):
                cb_copy(l, k, c, cb).start()

        def zero(c, _):
            accd[c] = jnp.zeros_like(accd[c])
            return 0

        lax.fori_loop(0, n, zero, 0)
        a = dot(hid[l, p, 0], wd[0])
        for f in range(1, FLOWS):
            a = a + dot(hid[l, p, f], wd[f])
        accd[p] = a
        finish(p)
        if l + 1 < layers:
            for f in order:
                up_copy(l + 1, f).wait()
                convert(st_up, wu, f, min(64, dl))
            if l + 2 < layers:
                for f in order:
                    up_copy(l + 2, f).start()

        def ag_step(s, _):
            for f in order:
                ag_arrival(l, f, s).wait_recv()

                @pl.when(s < n - 1)
                def _():
                    ag_copy(l, f, s + 1).start()

            cr, cl = wrap(p - s), wrap(p + s)
            h = FLOWS // 2
            accd[cr] += sum(dot(hid[l, cr, f], wd[f]) for f in range(h))
            accd[cl] += sum(dot(hid[l, cl, f], wd[f]) for f in range(h, FLOWS))

            @pl.when(s >= n // 2)
            def _():
                finish(cr)

            @pl.when(s > n // 2)
            def _():
                finish(cl)

            return 0

        lax.fori_loop(1, n, ag_step, 0)

        def gather_in(c):
            for k in range(1, m):
                cb_copy(l, k, c, lax.rem(cb + m - k, m)).wait_recv()
            b = cbb[l, 0, c].astype(f32)
            for k in range(1, m):
                b = b + cbb[l, k, c].astype(f32)
            b = b * ds[l : l + 1, :]
            bbuf[c] = b
            b = b * b
            t = b[:, :LANES]
            for j in range(1, dl // LANES):
                t = t + b[:, j * LANES : (j + 1) * LANES]
            ssq[c] = t

        def gather_pair(s, _):
            gather_in(wrap(p - s))
            gather_in(wrap(p + s))
            return 0

        gather_in(p)
        gather_in(wrap(p + n // 2))
        lax.fori_loop(n // 2 + 1, n, gather_pair, 0)

        t = jnp.transpose(ssq[...].reshape(tokens, LANES))
        t = jnp.sum(t, axis=0, keepdims=True)
        ssall[l, ra] = jnp.broadcast_to(t, (8, tokens))
        for k in range(1, n):
            ss_copy(l, k, ra).start()
        for k in range(1, n):
            ss_copy(l, k, lax.rem(ra + n - k, n)).wait_recv()
        t = ssall[l, 0]
        for k in range(1, n):
            t = t + ssall[l, k]
        t = lax.rsqrt(t / (dl * n) + norm_eps)
        t = jnp.broadcast_to(t[0:1, :], (LANES, tokens))
        ssq[...] = jnp.transpose(t).reshape(n, rows, LANES)

        before = tok if l == 0 else out

        def renew(c, _):
            inv = ssq[c]
            for j in range(dl // LANES):
                col = slice(j * LANES, (j + 1) * LANES)
                branch = bbuf[c, :, col] * inv * qg[l : l + 1, col]
                new = (residual_keep * before[c, :, col].astype(f32) + branch).astype(bf16)
                out[c, :, col] = new
                if l + 1 < layers:
                    xs[c, :, col] = (new.astype(f32) * pg[l + 1 : l + 2, col]).astype(bf16)
            return 0

        lax.fori_loop(0, n, renew, 0)

        def drain(s, _):
            for f in order:
                rs_copy(l, f, s).wait_send()
                ag_copy(l, f, s + 1).wait_send()
            return 0

        lax.fori_loop(0, n - 1, drain, 0)

        def drain_cb(c, _):
            for k in range(1, m):
                cb_copy(l, k, c, cb).wait_send()
            return 0

        lax.fori_loop(0, n, drain_cb, 0)
        for k in range(1, n):
            ss_copy(l, k, ra).wait_send()


def local(n, m, tokens, up_weight, up_scale, down_weight, down_scale, pre_gain, post_gain):
    t, dl = tokens.shape
    layers, _, fl = up_weight.shape
    fits = (
        n % 2 == 0 and n >= 4 and m >= 2 and t % (n * BF16_ROWS) == 0 and t % LANES == 0
        and fl % (FLOWS * LANES) == 0 and dl % LANES == 0
    )
    if not fits:
        return plain(
            tokens, up_weight, up_scale, down_weight, down_scale, pre_gain, post_gain
        )
    rows, fq = t // n, fl // FLOWS
    f32, bf16 = jnp.float32, jnp.bfloat16
    vmem = pl.BlockSpec(memory_space=pltpu.VMEM)
    hbm = pl.BlockSpec(memory_space=pl.ANY)
    dma = pltpu.SemaphoreType.DMA
    out = pl.pallas_call(
        functools.partial(kernel, n, m, layers),
        out_shape=jax.ShapeDtypeStruct((n, rows, dl), bf16),
        in_specs=[vmem, hbm, vmem, hbm, vmem, vmem, vmem],
        out_specs=vmem,
        scratch_shapes=[
            pltpu.VMEM((FLOWS, dl, fq), f32),
            pltpu.VMEM((FLOWS, fq, dl), f32),
            pltpu.VMEM((FLOWS, dl, fq), bf16),
            pltpu.VMEM((FLOWS, fq, dl), bf16),
            pltpu.VMEM((n, rows, dl), bf16),
            pltpu.VMEM((FLOWS, rows, fq), f32),
            pltpu.VMEM((FLOWS, n - 1, rows, fq), bf16),
            pltpu.VMEM((layers, FLOWS, n - 1, rows, fq), bf16),
            pltpu.VMEM((layers, n, FLOWS, rows, fq), bf16),
            pltpu.VMEM((n, rows, dl), f32),
            pltpu.VMEM((layers, m, n, rows, dl), bf16),
            pltpu.VMEM((n, rows, dl), f32),
            pltpu.VMEM((n, rows, LANES), f32),
            pltpu.VMEM((layers, n, 8, t), f32),
            dma((2, FLOWS)),
            dma((layers, FLOWS, n - 1)),
            dma((layers, FLOWS, n - 1)),
            dma((layers, FLOWS, n - 1)),
            dma((layers, FLOWS, n - 1)),
            dma((layers, m - 1, n)),
            dma((layers, m - 1, n)),
            dma((layers, n - 1)),
            dma((layers, n - 1)),
        ],
        compiler_params=pltpu.CompilerParams(
            collective_id=0, has_side_effects=True, vmem_limit_bytes=60 * 1024 * 1024
        ),
    )(
        tokens.reshape(n, rows, dl), up_weight, up_scale, down_weight, down_scale,
        pre_gain, post_gain,
    )
    return out.reshape(t, dl)


def solution(mesh):
    return jax.shard_map(
        functools.partial(local, mesh.shape["ra"], mesh.shape["cb"]),
        mesh=mesh,
        in_specs=(
            P(None, "ra"),
            P(None, "ra", "cb"),
            P(None, "cb"),
            P(None, "cb", "ra"),
            P(None, "ra"),
            P(None, "ra"),
            P(None, "ra"),
        ),
        out_specs=P(None, "ra"),
        check_vma=False,
    )
```

profile of v0, /device:TPU:0, one launch (start us, length us, event | category | flops | bytes accessed | tf_op | source)
XLA Modules:
  0.0 159.9 jit_solution(3243852443296518731)
XLA Ops:
  0.0 158.1 %shard_map.73 = bf16[8,48,512]{2,1,0:T(8,128)(2,1)} custom-call(bf16[8,48,512]{2,1,0:T(8,128)(2,1)} %bitcast.3, f32[2,512,4096]{2,1,0:T(8,128)} %up.1, f32[2,4096]{1,0:T(2,128)} %us.1, f32[2,4096,512]{2,1,0:T(8,128)} %dn.1, f32[2,512]{1,0:T(2,128)} %ds.1, f32[2,512]{1,0:T(2,128)} %pg.1, f32[2,512]{1,0:T(2,128)} %qg.1), custom_call_target="tpu_custom_call" | custom-call | tf_op jit(solution)/shard_map/pallas_call | solution.py:335
  158.1 1.8 %copy.9 = bf16[384,512]{1,0:T(8,128)(2,1)} copy(bf16[384,512]{1,0:T(8,128)(2,1)} %bitcast.2) | data formatting | bytes 786432
where the time goes:
time: 160 us
  Pallas kernels  158 us (99%)
  local copies, waits for them, and re-layouts  1.77 us (1%)
    pallas_call x1, Pallas kernels, local(): pl.pallas_call(functools.partial(kernel, n, m, layers), out_shape=jax.Sha...  158 us

commit v1 on v0

v1 whole, which is shorter than its diff:
```python
import functools

import jax
import jax.numpy as jnp
from jax import lax
from jax.experimental import pallas as pl
from jax.experimental.pallas import tpu as pltpu
from jax.sharding import PartitionSpec as P

norm_eps = 1e-06
residual_keep = 0.5
MESH = pl.DeviceIdType.MESH
STREAMS = 2
PIECES = 2
TAIL_IN_SCATTER = (1, 1, 2, 4, 5, 6)
TAIL_IN_GATHER = (0, 0, 1, 3, 4, 5)
LANES = 128
BF16_ROWS = 16


def plain(tokens, up_weight, up_scale, down_weight, down_scale, pre_gain, post_gain):
    values = tokens.astype(jnp.float32)
    model_width = tokens.shape[1] * lax.axis_size("ra")
    stream = tokens
    for sublayer in range(up_weight.shape[0]):
        scaled = (values * pre_gain[sublayer][None, :]).astype(jnp.bfloat16)
        up_matrix = up_weight[sublayer].astype(jnp.bfloat16)
        down_matrix = down_weight[sublayer].astype(jnp.bfloat16)
        partial_up = jnp.dot(scaled, up_matrix, preferred_element_type=jnp.float32)
        whole_up = lax.psum(partial_up.astype(jnp.bfloat16), "ra").astype(jnp.float32)
        hidden = jnp.square(jax.nn.relu(whole_up * up_scale[sublayer][None, :])).astype(
            jnp.bfloat16
        )
        partial_down = jnp.dot(hidden, down_matrix, preferred_element_type=jnp.float32)
        summed = lax.psum(partial_down.astype(jnp.bfloat16), "cb").astype(jnp.float32)
        branch_in = summed * down_scale[sublayer][None, :]
        post_squares = lax.psum(jnp.sum(branch_in * branch_in, axis=1), "ra")
        inv_post = lax.rsqrt(post_squares / model_width + norm_eps)[:, None]
        branch = branch_in * inv_post * post_gain[sublayer][None, :]
        stream = (residual_keep * values + branch).astype(jnp.bfloat16)
        values = stream.astype(jnp.float32)
    return stream


def kernel(
    n, m, layers,
    tok, up, us, dn, ds, pg, qg,
    out,
    st_up, st_dn, wu, wd, xs, own, sendb, recvb, hid, acc, core_s, core_r, pair, bbuf, ssq, ssall,
    w_sem, rs_s, rs_r, ag_s, ag_r, co_s, co_r, pr_s, pr_r, bs_s, bs_r, ss_s, ss_r,
):
    f32, bf16 = jnp.float32, jnp.bfloat16
    ra, cb = lax.axis_index("ra"), lax.axis_index("cb")
    rows = xs.shape[1]
    dl = tok.shape[1]
    fc = wu.shape[2]
    fh = fc // 2
    sub = rows // PIECES
    far = n // 2
    core, pairs = lax.rem(cb, 2), m // 2
    lane_rows = ssq.shape[0]

    def wrap(i):
        return lax.rem(i + 2 * n, n)

    half, odd = lax.div(ra, 2), lax.rem(ra, 2)
    p = half + odd * (n - 1 - 2 * half)

    def ra_of(q):
        hi = lax.div(q, n // 2)
        return 2 * q * (1 - hi) + hi * (2 * (n - 1 - q) + 1)

    target = [ra_of(wrap(p + 1)), ra_of(wrap(p - 1))]
    sign = [1, -1]
    long_flows = [(0, 0), (1, 1)]
    short_flows = [(0, 1), (1, 0)]
    flows = long_flows + short_flows

    def hops(d, e):
        return far if d == e else far - 1

    def chunk(q):
        return wrap(p + q)

    near_first = [0] + [q for k in range(1, far) for q in (k, -k)] + [far]
    far_first = near_first[::-1]

    def up_copy(l, i):
        c = chunk(far_first[i])
        return pltpu.make_async_copy(
            up.at[l, :, pl.ds(pl.multiple_of(c * fc, fc), fc)], st_up.at[i], w_sem.at[0, i]
        )

    def dn_copy(l, i):
        c = chunk(near_first[i])
        return pltpu.make_async_copy(
            dn.at[l, pl.ds(pl.multiple_of(c * fc, fc), fc), :], st_dn.at[i], w_sem.at[1, i]
        )

    def convert(src, dst, i, c):
        block = 32

        def body(j, _):
            r = pl.ds(pl.multiple_of(j * block, block), block)
            dst[c, r, :] = src[i, r, :].astype(bf16)
            return 0

        lax.fori_loop(0, src.shape[1] // block, body, 0)

    def take_up(l, chosen):
        for i in chosen:
            up_copy(l, i).wait()
            convert(st_up, wu, i, chunk(far_first[i]))
            if l + 1 < layers:
                up_copy(l + 1, i).start()

    def take_dn(l, chosen):
        for i in chosen:
            dn_copy(l, i).wait()
            convert(st_dn, wd, i, chunk(near_first[i]))
            if l + 1 < layers:
                dn_copy(l + 1, i).start()

    def part(h):
        return pl.ds(h * sub, sub)

    def rs_copy(l, g, d, e, j, h):
        return pltpu.make_async_remote_copy(
            src_ref=sendb.at[g, d, e, j, part(h), :],
            dst_ref=recvb.at[l, g, d, e, j, part(h), :],
            send_sem=rs_s.at[l, g, d, e, j, h], recv_sem=rs_r.at[l, g, d, e, j, h],
            device_id={"ra": target[d]}, device_id_type=MESH,
        )

    def ag_copy(l, g, d, e, s, h, arriving=False):
        c = chunk(-sign[d] * (s if arriving else s - 1))
        piece = hid.at[l, g, c, e, part(h), :]
        return pltpu.make_async_remote_copy(
            src_ref=piece, dst_ref=piece,
            send_sem=ag_s.at[l, g, d, e, s - 1, h], recv_sem=ag_r.at[l, g, d, e, s - 1, h],
            device_id={"ra": target[d]}, device_id_type=MESH,
        )

    def core_copy(l, g):
        return pltpu.make_async_remote_copy(
            src_ref=core_s.at[l, g], dst_ref=core_r.at[l, g],
            send_sem=co_s.at[l, g], recv_sem=co_r.at[l, g],
            device_id={"cb": cb + 1 - 2 * core}, device_id_type=MESH,
        )

    def pair_copy(l, g, k, who):
        return pltpu.make_async_remote_copy(
            src_ref=pair.at[l, g, who], dst_ref=pair.at[l, g, who],
            send_sem=pr_s.at[l, g, k - 1], recv_sem=pr_r.at[l, g, k - 1],
            device_id={"cb": lax.rem(cb + 2 * k, m)}, device_id_type=MESH,
        )

    def branch_copy(l, g, who):
        return pltpu.make_async_remote_copy(
            src_ref=bbuf.at[l, g, who], dst_ref=bbuf.at[l, g, who],
            send_sem=bs_s.at[l, g], recv_sem=bs_r.at[l, g],
            device_id={"cb": cb + 1 - 2 * core}, device_id_type=MESH,
        )

    def ss_copy(l, g, k, who):
        return pltpu.make_async_remote_copy(
            src_ref=ssall.at[l, g, who], dst_ref=ssall.at[l, g, who],
            send_sem=ss_s.at[l, g, k - 1], recv_sem=ss_r.at[l, g, k - 1],
            device_id={"ra": lax.rem(ra + k, n)}, device_id_type=MESH,
        )

    def dot(a, b):
        return jnp.dot(a, b, preferred_element_type=f32)

    def project(g, q):
        c = chunk(q)
        own[g, c] = dot(xs[g], wu[c])

    def mine(g, q, e, h):
        return own[g, chunk(q), h * sub : (h + 1) * sub, e * fh : (e + 1) * fh]

    def scatter(l, g, k, which):
        for h in range(PIECES):
            for d, e in which:
                j = k if d == e else k - 1
                v = mine(g, sign[d] * (far - k), e, h)
                if j > 0:
                    rs_copy(l, g, d, e, j - 1, h).wait_recv()
                    v = v + recvb[l, g, d, e, j - 1, part(h), :].astype(f32)
                sendb[g, d, e, j, part(h), :] = v.astype(bf16)
                rs_copy(l, g, d, e, j, h).start()

    def activate(l, g):
        project(g, 0)
        for e in (0, 1):
            scale = us[l : l + 1, pl.ds(pl.multiple_of(p * fc + e * fh, fh), fh)]
            for h in range(PIECES):
                v = mine(g, 0, e, h)
                for d in (0, 1):
                    j = hops(d, e) - 1
                    rs_copy(l, g, d, e, j, h).wait_recv()
                    v = v + recvb[l, g, d, e, j, part(h), :].astype(f32)
                v = jnp.maximum(v * scale, 0.0)
                hid[l, g, p, e, part(h), :] = (v * v).astype(bf16)

    def forward(l, g, s, which):
        for h in range(PIECES):
            for d, e in which:
                if s > 1:
                    ag_copy(l, g, d, e, s - 1, h, arriving=True).wait_recv()
                if s <= hops(d, e):
                    ag_copy(l, g, d, e, s, h).start()

    def reduce_hidden(l, g, q, first=False):
        c = chunk(q)
        a = dot(hid[l, g, c, 0], wd[c, :fh, :]) + dot(hid[l, g, c, 1], wd[c, fh:, :])
        if first:
            acc[g] = a
        else:
            acc[g] += a

    mid = rows // 2

    def share_cores(l, g):
        core_s[l, g] = acc[g, pl.ds(pl.multiple_of((1 - core) * mid, mid), mid), :].astype(bf16)
        core_copy(l, g).start()

    def share_pairs(l, g):
        y = lax.div(cb, 2)
        kept = acc[g, pl.ds(pl.multiple_of(core * mid, mid), mid), :].astype(bf16).astype(f32)
        core_copy(l, g).wait_recv()
        pair[l, g, y] = (kept + core_r[l, g].astype(f32)).astype(bf16)
        for k in range(1, pairs):
            pair_copy(l, g, k, y).start()

    def squares(l, g, who):
        b = bbuf[l, g, who]
        b = b * b
        t = b[:, :LANES]
        for j in range(1, dl // LANES):
            t = t + b[:, j * LANES : (j + 1) * LANES]
        ssq[pl.ds(pl.multiple_of(who * mid, mid), mid), :] = t

    def share_branch(l, g):
        y = lax.div(cb, 2)
        for k in range(1, pairs):
            pair_copy(l, g, k, lax.rem(y + pairs - k, pairs)).wait_recv()
        b = pair[l, g, 0].astype(f32)
        for k in range(1, pairs):
            b = b + pair[l, g, k].astype(f32)
        bbuf[l, g, core] = b * ds[l : l + 1, :]
        branch_copy(l, g, core).start()
        squares(l, g, core)

    def share_squares(l, g):
        branch_copy(l, g, 1 - core).wait_recv()
        squares(l, g, 1 - core)
        t = jnp.sum(jnp.transpose(ssq[...]), axis=0, keepdims=True)
        ssall[l, g, ra] = jnp.broadcast_to(t, (8, lane_rows))
        for k in range(1, n):
            ss_copy(l, g, k, ra).start()

    def renew(l, g):
        for k in range(1, n):
            ss_copy(l, g, k, lax.rem(ra + n - k, n)).wait_recv()
        t = ssall[l, g, 0]
        for k in range(1, n):
            t = t + ssall[l, g, k]
        t = lax.rsqrt(t / (dl * n) + norm_eps)
        ssq[...] = jnp.transpose(jnp.broadcast_to(t[0:1, :], (LANES, lane_rows)))
        before = tok if l == 0 else out
        for who in (0, 1):
            inv = ssq[who * mid : (who + 1) * mid, :]
            at = slice(g * rows + who * mid, g * rows + (who + 1) * mid)
            for j in range(dl // LANES):
                col = slice(j * LANES, (j + 1) * LANES)
                branch = bbuf[l, g, who, :, col] * inv * qg[l : l + 1, col]
                new = (residual_keep * before[at, col].astype(f32) + branch).astype(bf16)
                out[at, col] = new
                if l + 1 < layers:
                    xs[g, who * mid : (who + 1) * mid, col] = (
                        new.astype(f32) * pg[l + 1 : l + 2, col]
                    ).astype(bf16)

    def drain_scatter(l, g):
        for d, e in flows:
            for j in range(hops(d, e)):
                for h in range(PIECES):
                    rs_copy(l, g, d, e, j, h).wait_send()

    def drain_rest(l, g):
        for d, e in flows:
            for s in range(1, hops(d, e) + 1):
                for h in range(PIECES):
                    ag_copy(l, g, d, e, s, h).wait_send()
        core_copy(l, g).wait_send()
        for k in range(1, pairs):
            pair_copy(l, g, k, lax.div(cb, 2)).wait_send()
        branch_copy(l, g, core).wait_send()
        for k in range(1, n):
            ss_copy(l, g, k, ra).wait_send()

    for i in range(n):
        up_copy(0, i).start()

    barrier = pltpu.get_barrier_semaphore()
    for k in range(1, n):
        pl.semaphore_signal(
            barrier, inc=1, device_id={"ra": lax.rem(ra + k, n)}, device_id_type=MESH
        )
    for k in range(1, m):
        pl.semaphore_signal(
            barrier, inc=1, device_id={"cb": lax.rem(cb + k, m)}, device_id_type=MESH
        )

    for g in range(STREAMS):
        xs[g] = (tok[g * rows : (g + 1) * rows, :].astype(f32) * pg[0:1, :]).astype(bf16)
    ssq[...] = jnp.zeros_like(ssq)

    def tail_steps(l, g):
        def end():
            forward(l, g, far + 1, long_flows)
            reduce_hidden(l, g, far)
            share_cores(l, g)

        def short_end():
            forward(l, g, far, short_flows)
            reduce_hidden(l, g, far - 1)
            reduce_hidden(l, g, 1 - far)

        return [
            short_end, end, lambda: share_pairs(l, g), lambda: share_branch(l, g),
            lambda: share_squares(l, g), lambda: renew(l, g),
        ]

    def scatter_steps(l, g):
        fresh = l == 0 and g == 0

        def first():
            if fresh:
                take_up(l, [0])
            project(g, far)
            if fresh:
                pl.semaphore_wait(barrier, n + m - 2)
            scatter(l, g, 0, long_flows)

        def short(k):
            if fresh:
                take_up(l, [2 * k - 1, 2 * k])
                if k == 1:
                    for i in range(n):
                        dn_copy(l, i).start()
                if k == far - 1:
                    take_up(l, [n - 1])
            project(g, far - k)
            project(g, k - far)
            scatter(l, g, k, short_flows)

        steps = [first]
        for k in range(1, far):
            steps.append(functools.partial(short, k))
            steps.append(functools.partial(scatter, l, g, k, long_flows))
        return steps

    def gather_steps(l, g):
        def begin():
            forward(l, g, 1, flows)
            reduce_hidden(l, g, 0, first=True)

        def short(s):
            forward(l, g, s, short_flows)
            reduce_hidden(l, g, s - 1)
            reduce_hidden(l, g, 1 - s)

        steps = [begin]
        for s in range(2, far + 1):
            steps.append(functools.partial(forward, l, g, s, long_flows))
            if s < far:
                steps.append(functools.partial(short, s))
        return steps

    def run(steps, side, slots):
        slots = [min(at, len(steps) - 1) for at in slots]
        for i, step in enumerate(steps):
            step()
            for extra, at in zip(side, slots):
                if at == i:
                    extra()

    pending, first_half, second_half = [], range(n // 2), range(n // 2, n)
    for l in range(layers):
        run(scatter_steps(l, 0), pending, TAIL_IN_SCATTER)
        run(
            scatter_steps(l, 1),
            [
                lambda: activate(l, 0), lambda: take_dn(l, first_half),
                lambda: take_dn(l, second_half),
            ],
            (1, 2, 3),
        )
        side = [lambda: activate(l, 1), lambda: drain_scatter(l, 0)]
        if l + 1 < layers:
            side += [
                lambda: take_up(l + 1, first_half), lambda: take_up(l + 1, second_half)
            ]
        run(gather_steps(l, 0), side, (0, 4, 2, 3))
        run(
            gather_steps(l, 1), tail_steps(l, 0) + [lambda: drain_scatter(l, 1)],
            TAIL_IN_GATHER + (4,),
        )
        pending = tail_steps(l, 1)
    for step in pending:
        step()
    for l in range(layers):
        for g in range(STREAMS):
            drain_rest(l, g)


def local(n, m, tokens, up_weight, up_scale, down_weight, down_scale, pre_gain, post_gain):
    t, dl = tokens.shape
    layers, _, fl = up_weight.shape
    fits = (
        n % 2 == 0 and n >= 4 and m % 2 == 0 and t % (STREAMS * PIECES * BF16_ROWS) == 0
        and t % (STREAMS * 2 * BF16_ROWS) == 0 and fl % (2 * n * LANES) == 0
        and dl % LANES == 0
    )
    if not fits:
        return plain(
            tokens, up_weight, up_scale, down_weight, down_scale, pre_gain, post_gain
        )
    rows, fc, far = t // STREAMS, fl // n, n // 2
    lane_rows = -(-rows // LANES) * LANES
    f32, bf16 = jnp.float32, jnp.bfloat16
    vmem = pl.BlockSpec(memory_space=pltpu.VMEM)
    hbm = pl.BlockSpec(memory_space=pl.ANY)
    dma = pltpu.SemaphoreType.DMA
    return pl.pallas_call(
        functools.partial(kernel, n, m, layers),
        out_shape=jax.ShapeDtypeStruct((t, dl), bf16),
        in_specs=[vmem, hbm, vmem, hbm, vmem, vmem, vmem],
        out_specs=vmem,
        scratch_shapes=[
            pltpu.VMEM((n, dl, fc), f32),
            pltpu.VMEM((n, fc, dl), f32),
            pltpu.VMEM((n, dl, fc), bf16),
            pltpu.VMEM((n, fc, dl), bf16),
            pltpu.VMEM((STREAMS, rows, dl), bf16),
            pltpu.VMEM((STREAMS, n, rows, fc), f32),
            pltpu.VMEM((STREAMS, 2, 2, far, rows, fc // 2), bf16),
            pltpu.VMEM((layers, STREAMS, 2, 2, far, rows, fc // 2), bf16),
            pltpu.VMEM((layers, STREAMS, n, 2, rows, fc // 2), bf16),
            pltpu.VMEM((STREAMS, rows, dl), f32),
            pltpu.VMEM((layers, STREAMS, rows // 2, dl), bf16),
            pltpu.VMEM((layers, STREAMS, rows // 2, dl), bf16),
            pltpu.VMEM((layers, STREAMS, m // 2, rows // 2, dl), bf16),
            pltpu.VMEM((layers, STREAMS, 2, rows // 2, dl), f32),
            pltpu.VMEM((lane_rows, LANES), f32),
            pltpu.VMEM((layers, STREAMS, n, 8, lane_rows), f32),
            dma((2, n)),
            dma((layers, STREAMS, 2, 2, far, PIECES)),
            dma((layers, STREAMS, 2, 2, far, PIECES)),
            dma((layers, STREAMS, 2, 2, far, PIECES)),
            dma((layers, STREAMS, 2, 2, far, PIECES)),
            dma((layers, STREAMS)),
            dma((layers, STREAMS)),
            dma((layers, STREAMS, max(m // 2 - 1, 1))),
            dma((layers, STREAMS, max(m // 2 - 1, 1))),
            dma((layers, STREAMS)),
            dma((layers, STREAMS)),
            dma((layers, STREAMS, n - 1)),
            dma((layers, STREAMS, n - 1)),
        ],
        compiler_params=pltpu.CompilerParams(
            collective_id=0, has_side_effects=True, vmem_limit_bytes=60 * 1024 * 1024
        ),
    )(tokens, up_weight, up_scale, down_weight, down_scale, pre_gain, post_gain)


def solution(mesh):
    return jax.shard_map(
        functools.partial(local, mesh.shape["ra"], mesh.shape["cb"]),
        mesh=mesh,
        in_specs=(
            P(None, "ra"),
            P(None, "ra", "cb"),
            P(None, "cb"),
            P(None, "cb", "ra"),
            P(None, "ra"),
            P(None, "ra"),
            P(None, "ra"),
        ),
        out_specs=P(None, "ra"),
        check_vma=False,
    )
```

time: 160 us -> 151 us (0.944)
  Pallas kernels: 158 us -> 149 us
    pallas_call x1, Pallas kernels: 158 us -> 149 us  [local(): pl.pallas_call(functools.partial(kernel, n, m, layers), out_shape=jax.Sha...]
where the time goes in v1:
time: 151 us
  Pallas kernels  149 us (99%)
  local copies, waits for them, and re-layouts  1.77 us (1%)
    pallas_call x1, Pallas kernels, local(): pl.pallas_call(functools.partial(kernel, n, m, layers), out_shape=jax.Sha...  149 us

profile of v1, /device:TPU:0, one launch (start us, length us, event | category | flops | bytes accessed | tf_op | source)
XLA Modules:
  0.0 150.6 jit_solution(12163554356671738052)
XLA Ops:
  0.0 148.8 %shard_map.73 = bf16[384,512]{1,0:T(8,128)(2,1)} custom-call(bf16[384,512]{1,0:T(8,128)(2,1)} %tok.1, f32[2,512,4096]{2,1,0:T(8,128)} %up.1, f32[2,4096]{1,0:T(2,128)} %us.1, f32[2,4096,512]{2,1,0:T(8,128)} %dn.1, f32[2,512]{1,0:T(2,128)} %ds.1, f32[2,512]{1,0:T(2,128)} %pg.1, f32[2,512]{1,0:T(2,128)} %qg.1), custom_call_target="tpu_custom_call" | custom-call | tf_op jit(solution)/shard_map/pallas_call | solution.py:437
  148.8 1.8 %copy.9 = bf16[384,512]{1,0:T(8,128)(2,1)} copy(bf16[384,512]{1,0:T(8,128)(2,1)} %shard_map.73) | data formatting | bytes 786432

commit v2 on v1

--- a/solution.py
+++ b/solution.py
@@ -12,8 +12,8 @@
 MESH = pl.DeviceIdType.MESH
 STREAMS = 2
 PIECES = 2
-TAIL_IN_SCATTER = (1, 1, 2, 4, 5, 6)
-TAIL_IN_GATHER = (0, 0, 1, 3, 4, 5)
+TAIL_IN_SCATTER = (1, 1, 3, 6)
+TAIL_IN_GATHER = (0, 0, 2, 5)
 LANES = 128
 BF16_ROWS = 16
 
@@ -44,10 +44,11 @@
 
 def kernel(
     n, m, layers,
-    tok, up, us, dn, ds, pg, qg,
+    tok_in, up, us_in, dn, ds_in, pg_in, qg_in,
     out,
-    st_up, st_dn, wu, wd, xs, own, sendb, recvb, hid, acc, core_s, core_r, pair, bbuf, ssq, ssall,
-    w_sem, rs_s, rs_r, ag_s, ag_r, co_s, co_r, pr_s, pr_r, bs_s, bs_r, ss_s, ss_r,
+    st_up, st_dn, wu, wd, xs, own, sendb, recvb, hid, acc, part_s, part_r, sums, ssq, ssall,
+    tok, us, ds, pg, qg,
+    w_sem, in_sem, rs_s, rs_r, ag_s, ag_r, pa_s, pa_r, su_s, su_r, ss_s, ss_r,
 ):
     f32, bf16 = jnp.float32, jnp.bfloat16
     ra, cb = lax.axis_index("ra"), lax.axis_index("cb")
@@ -57,8 +58,6 @@
     fh = fc // 2
     sub = rows // PIECES
     far = n // 2
-    core, pairs = lax.rem(cb, 2), m // 2
-    lane_rows = ssq.shape[0]
 
     def wrap(i):
         return lax.rem(i + 2 * n, n)
@@ -141,32 +140,27 @@
             device_id={"ra": target[d]}, device_id_type=MESH,
         )
 
-    def core_copy(l, g):
+    def part_copy(l, g, k):
         return pltpu.make_async_remote_copy(
-            src_ref=core_s.at[l, g], dst_ref=core_r.at[l, g],
-            send_sem=co_s.at[l, g], recv_sem=co_r.at[l, g],
-            device_id={"cb": cb + 1 - 2 * core}, device_id_type=MESH,
-        )
-
-    def pair_copy(l, g, k, who):
+            src_ref=part_s.at[l, g, lax.rem(cb + k, m)], dst_ref=part_r.at[l, g, k - 1],
+            send_sem=pa_s.at[l, g, k - 1], recv_sem=pa_r.at[l, g, k - 1],
+            device_id={"cb": lax.rem(cb + k, m)}, device_id_type=MESH,
+        )
+
+    def sum_copy(l, g, k, who):
         return pltpu.make_async_remote_copy(
-            src_ref=pair.at[l, g, who], dst_ref=pair.at[l, g, who],
-            send_sem=pr_s.at[l, g, k - 1], recv_sem=pr_r.at[l, g, k - 1],
-            device_id={"cb": lax.rem(cb + 2 * k, m)}, device_id_type=MESH,
-        )
-
-    def branch_copy(l, g, who):
+            src_ref=sums.at[l, g, who], dst_ref=sums.at[l, g, who],
+            send_sem=su_s.at[l, g, k - 1], recv_sem=su_r.at[l, g, k - 1],
+            device_id={"cb": lax.rem(cb + k, m)}, device_id_type=MESH,
+        )
+
+    def ss_copy(l, g, i, k, arriving=False):
+        a, b = (lax.rem(ra + n - i, n), lax.rem(cb + m - k, m)) if arriving else (ra, cb)
         return pltpu.make_async_remote_copy(
-            src_ref=bbuf.at[l, g, who], dst_ref=bbuf.at[l, g, who],
-            send_sem=bs_s.at[l, g], recv_sem=bs_r.at[l, g],
-            device_id={"cb": cb + 1 - 2 * core}, device_id_type=MESH,
-        )
-
-    def ss_copy(l, g, k, who):
-        return pltpu.make_async_remote_copy(
-            src_ref=ssall.at[l, g, who], dst_ref=ssall.at[l, g, who],
-            send_sem=ss_s.at[l, g, k - 1], recv_sem=ss_r.at[l, g, k - 1],
-            device_id={"ra": lax.rem(ra + k, n)}, device_id_type=MESH,
+            src_ref=ssall.at[l, g, b, a], dst_ref=ssall.at[l, g, b, a],
+            send_sem=ss_s.at[l, g, i * m + k - 1], recv_sem=ss_r.at[l, g, i * m + k - 1],
+            device_id={"ra": lax.rem(ra + i, n), "cb": lax.rem(cb + k, m)},
+            device_id_type=MESH,
         )
 
     def dot(a, b):
@@ -219,66 +213,55 @@
         else:
             acc[g] += a
 
-    mid = rows // 2
-
-    def share_cores(l, g):
-        core_s[l, g] = acc[g, pl.ds(pl.multiple_of((1 - core) * mid, mid), mid), :].astype(bf16)
-        core_copy(l, g).start()
-
-    def share_pairs(l, g):
-        y = lax.div(cb, 2)
-        kept = acc[g, pl.ds(pl.multiple_of(core * mid, mid), mid), :].astype(bf16).astype(f32)
-        core_copy(l, g).wait_recv()
-        pair[l, g, y] = (kept + core_r[l, g].astype(f32)).astype(bf16)
-        for k in range(1, pairs):
-            pair_copy(l, g, k, y).start()
-
-    def squares(l, g, who):
-        b = bbuf[l, g, who]
+    quarter = rows // m
+    others = [(i, k) for i in range(n) for k in range(m) if i or k]
+
+    def share_parts(l, g):
+        for who in range(m):
+            part_s[l, g, who] = acc[g, who * quarter : (who + 1) * quarter, :].astype(bf16)
+        for k in range(1, m):
+            part_copy(l, g, k).start()
+
+    def share_sums(l, g):
+        v = part_s[l, g, cb].astype(f32)
+        for k in range(1, m):
+            part_copy(l, g, k).wait_recv()
+            v = v + part_r[l, g, k - 1].astype(f32)
+        v = v.astype(bf16)
+        sums[l, g, cb] = v
+        for k in range(1, m):
+            sum_copy(l, g, k, cb).start()
+        b = v.astype(f32) * ds[l : l + 1, :]
         b = b * b
         t = b[:, :LANES]
         for j in range(1, dl // LANES):
             t = t + b[:, j * LANES : (j + 1) * LANES]
-        ssq[pl.ds(pl.multiple_of(who * mid, mid), mid), :] = t
-
-    def share_branch(l, g):
-        y = lax.div(cb, 2)
-        for k in range(1, pairs):
-            pair_copy(l, g, k, lax.rem(y + pairs - k, pairs)).wait_recv()
-        b = pair[l, g, 0].astype(f32)
-        for k in range(1, pairs):
-            b = b + pair[l, g, k].astype(f32)
-        bbuf[l, g, core] = b * ds[l : l + 1, :]
-        branch_copy(l, g, core).start()
-        squares(l, g, core)
-
-    def share_squares(l, g):
-        branch_copy(l, g, 1 - core).wait_recv()
-        squares(l, g, 1 - core)
-        t = jnp.sum(jnp.transpose(ssq[...]), axis=0, keepdims=True)
-        ssall[l, g, ra] = jnp.broadcast_to(t, (8, lane_rows))
-        for k in range(1, n):
-            ss_copy(l, g, k, ra).start()
+        ssq[:quarter, :] = t
+        ssall[l, g, cb, ra] = jnp.sum(jnp.transpose(ssq[...]), axis=0, keepdims=True)
+        for i, k in others:
+            ss_copy(l, g, i, k).start()
 
     def renew(l, g):
-        for k in range(1, n):
-            ss_copy(l, g, k, lax.rem(ra + n - k, n)).wait_recv()
-        t = ssall[l, g, 0]
-        for k in range(1, n):
-            t = t + ssall[l, g, k]
-        t = lax.rsqrt(t / (dl * n) + norm_eps)
-        ssq[...] = jnp.transpose(jnp.broadcast_to(t[0:1, :], (LANES, lane_rows)))
+        for k in range(1, m):
+            sum_copy(l, g, k, lax.rem(cb + m - k, m)).wait_recv()
+        for i, k in others:
+            ss_copy(l, g, i, k, arriving=True).wait_recv()
         before = tok if l == 0 else out
-        for who in (0, 1):
-            inv = ssq[who * mid : (who + 1) * mid, :]
-            at = slice(g * rows + who * mid, g * rows + (who + 1) * mid)
+        for who in range(m):
+            t = ssall[l, g, who, 0]
+            for i in range(1, n):
+                t = t + ssall[l, g, who, i]
+            t = lax.rsqrt(t / (dl * n) + norm_eps)
+            inv = jnp.transpose(jnp.broadcast_to(t, (LANES, ssq.shape[0])))[:quarter, :]
+            at = slice(g * rows + who * quarter, g * rows + (who + 1) * quarter)
             for j in range(dl // LANES):
                 col = slice(j * LANES, (j + 1) * LANES)
-                branch = bbuf[l, g, who, :, col] * inv * qg[l : l + 1, col]
+                b = sums[l, g, who, :, col].astype(f32) * ds[l : l + 1, col]
+                branch = b * inv * qg[l : l + 1, col]
                 new = (residual_keep * before[at, col].astype(f32) + branch).astype(bf16)
                 out[at, col] = new
                 if l + 1 < layers:
-                    xs[g, who * mid : (who + 1) * mid, col] = (
+                    xs[g, who * quarter : (who + 1) * quarter, col] = (
                         new.astype(f32) * pg[l + 1 : l + 2, col]
                     ).astype(bf16)
 
@@ -293,35 +276,43 @@
             for s in range(1, hops(d, e) + 1):
                 for h in range(PIECES):
                     ag_copy(l, g, d, e, s, h).wait_send()
-        core_copy(l, g).wait_send()
-        for k in range(1, pairs):
-            pair_copy(l, g, k, lax.div(cb, 2)).wait_send()
-        branch_copy(l, g, core).wait_send()
-        for k in range(1, n):
-            ss_copy(l, g, k, ra).wait_send()
-
-    for i in range(n):
-        up_copy(0, i).start()
+        for k in range(1, m):
+            part_copy(l, g, k).wait_send()
+            sum_copy(l, g, k, cb).wait_send()
+        for i, k in others:
+            ss_copy(l, g, i, k).wait_send()
 
     barrier = pltpu.get_barrier_semaphore()
-    for k in range(1, n):
+    for d in (0, 1):
         pl.semaphore_signal(
-            barrier, inc=1, device_id={"ra": lax.rem(ra + k, n)}, device_id_type=MESH
+            barrier, inc=1, device_id={"ra": target[d]}, device_id_type=MESH
         )
     for k in range(1, m):
         pl.semaphore_signal(
             barrier, inc=1, device_id={"cb": lax.rem(cb + k, m)}, device_id_type=MESH
         )
 
+    inputs = [
+        pltpu.make_async_copy(src, dst, in_sem.at[i])
+        for i, (src, dst) in enumerate(
+            [(pg_in, pg), (tok_in, tok), (us_in, us), (ds_in, ds), (qg_in, qg)]
+        )
+    ]
+    for copy in inputs:
+        copy.start()
+    for i in range(n):
+        up_copy(0, i).start()
+    ssq[...] = jnp.zeros_like(ssq)
+    for copy in inputs:
+        copy.wait()
     for g in range(STREAMS):
         xs[g] = (tok[g * rows : (g + 1) * rows, :].astype(f32) * pg[0:1, :]).astype(bf16)
-    ssq[...] = jnp.zeros_like(ssq)
 
     def tail_steps(l, g):
         def end():
             forward(l, g, far + 1, long_flows)
             reduce_hidden(l, g, far)
-            share_cores(l, g)
+            share_parts(l, g)
 
         def short_end():
             forward(l, g, far, short_flows)
@@ -329,8 +320,7 @@
             reduce_hidden(l, g, 1 - far)
 
         return [
-            short_end, end, lambda: share_pairs(l, g), lambda: share_branch(l, g),
-            lambda: share_squares(l, g), lambda: renew(l, g),
+            short_end, end, lambda: share_sums(l, g), lambda: renew(l, g),
         ]
 
     def scatter_steps(l, g):
@@ -341,7 +331,7 @@
                 take_up(l, [0])
             project(g, far)
             if fresh:
-                pl.semaphore_wait(barrier, n + m - 2)
+                pl.semaphore_wait(barrier, m + 1)
             scatter(l, g, 0, long_flows)
 
         def short(k):
@@ -364,7 +354,8 @@
 
     def gather_steps(l, g):
         def begin():
-            forward(l, g, 1, flows)
+            forward(l, g, 1, long_flows)
+            forward(l, g, 1, short_flows)
             reduce_hidden(l, g, 0, first=True)
 
         def short(s):
@@ -420,8 +411,8 @@
     t, dl = tokens.shape
     layers, _, fl = up_weight.shape
     fits = (
-        n % 2 == 0 and n >= 4 and m % 2 == 0 and t % (STREAMS * PIECES * BF16_ROWS) == 0
-        and t % (STREAMS * 2 * BF16_ROWS) == 0 and fl % (2 * n * LANES) == 0
+        n % 2 == 0 and n >= 4 and m >= 2 and t % (STREAMS * PIECES * BF16_ROWS) == 0
+        and t % (STREAMS * m * BF16_ROWS) == 0 and fl % (2 * n * LANES) == 0
         and dl % LANES == 0
     )
     if not fits:
@@ -429,15 +420,15 @@
             tokens, up_weight, up_scale, down_weight, down_scale, pre_gain, post_gain
         )
     rows, fc, far = t // STREAMS, fl // n, n // 2
-    lane_rows = -(-rows // LANES) * LANES
+    lane_rows = -(-(rows // m) // LANES) * LANES
     f32, bf16 = jnp.float32, jnp.bfloat16
     vmem = pl.BlockSpec(memory_space=pltpu.VMEM)
-    hbm = pl.BlockSpec(memory_space=pl.ANY)
+    hbm = pl.BlockSpec(memory_space=pltpu.HBM)
     dma = pltpu.SemaphoreType.DMA
     return pl.pallas_call(
         functools.partial(kernel, n, m, layers),
-        out_shape=jax.ShapeDtypeStruct((t, dl), bf16),
-        in_specs=[vmem, hbm, vmem, hbm, vmem, vmem, vmem],
+        out_shape=pltpu.VMEM((t, dl), bf16),
+        in_specs=[hbm] * 7,
         out_specs=vmem,
         scratch_shapes=[
             pltpu.VMEM((n, dl, fc), f32),
@@ -450,25 +441,28 @@
             pltpu.VMEM((layers, STREAMS, 2, 2, far, rows, fc // 2), bf16),
             pltpu.VMEM((layers, STREAMS, n, 2, rows, fc // 2), bf16),
             pltpu.VMEM((STREAMS, rows, dl), f32),
-            pltpu.VMEM((layers, STREAMS, rows // 2, dl), bf16),
-            pltpu.VMEM((layers, STREAMS, rows // 2, dl), bf16),
-            pltpu.VMEM((layers, STREAMS, m // 2, rows // 2, dl), bf16),
-            pltpu.VMEM((layers, STREAMS, 2, rows // 2, dl), f32),
+            pltpu.VMEM((layers, STREAMS, m, rows // m, dl), bf16),
+            pltpu.VMEM((layers, STREAMS, m - 1, rows // m, dl), bf16),
+            pltpu.VMEM((layers, STREAMS, m, rows // m, dl), bf16),
             pltpu.VMEM((lane_rows, LANES), f32),
-            pltpu.VMEM((layers, STREAMS, n, 8, lane_rows), f32),
+            pltpu.VMEM((layers, STREAMS, m, n, 1, lane_rows), f32),
+            pltpu.VMEM((t, dl), bf16),
+            pltpu.VMEM(up_scale.shape, f32),
+            pltpu.VMEM(down_scale.shape, f32),
+            pltpu.VMEM(pre_gain.shape, f32),
+            pltpu.VMEM(post_gain.shape, f32),
             dma((2, n)),
+            dma((5,)),
             dma((layers, STREAMS, 2, 2, far, PIECES)),
             dma((layers, STREAMS, 2, 2, far, PIECES)),
             dma((layers, STREAMS, 2, 2, far, PIECES)),
             dma((layers, STREAMS, 2, 2, far, PIECES)),
-            dma((layers, STREAMS)),
-            dma((layers, STREAMS)),
-            dma((layers, STREAMS, max(m // 2 - 1, 1))),
-            dma((layers, STREAMS, max(m // 2 - 1, 1))),
-            dma((layers, STREAMS)),
-            dma((layers, STREAMS)),
-            dma((layers, STREAMS, n - 1)),
-            dma((layers, STREAMS, n - 1)),
+            dma((layers, STREAMS, m - 1)),
+            dma((layers, STREAMS, m - 1)),
+            dma((layers, STREAMS, m - 1)),
+            dma((layers, STREAMS, m - 1)),
+            dma((layers, STREAMS, n * m - 1)),
+            dma((layers, STREAMS, n * m - 1)),
         ],
         compiler_params=pltpu.CompilerParams(
             collective_id=0, has_side_effects=True, vmem_limit_bytes=60 * 1024 * 1024

time: 151 us -> 144 us (0.954)
  Pallas kernels: 149 us -> 143 us
    pallas_call x1, Pallas kernels: 149 us -> 143 us  [local(): pl.pallas_call(functools.partial(kernel, n, m, layers), out_shape=pltpu.V...]
where the time goes in v2:
time: 144 us
  Pallas kernels  143 us (99%)
    pallas_call x1, Pallas kernels, local(): pl.pallas_call(functools.partial(kernel, n, m, layers), out_shape=pltpu.V...  143 us

profile of v2, /device:TPU:0, one launch (start us, length us, event | category | flops | bytes accessed | tf_op | source)
XLA Modules:
  0.0 144.0 jit_solution(16162869343696793329)
XLA Ops:
  0.0 143.2 %shard_map.73 = bf16[384,512]{1,0:T(8,128)(2,1)S(1)} custom-call(bf16[384,512]{1,0:T(8,128)(2,1)} %tok_in.1, f32[2,512,4096]{2,1,0:T(8,128)} %up.1, f32[2,4096]{1,0:T(2,128)} %us_in.1, f32[2,4096,512]{2,1,0:T(8,128)} %dn.1, f32[2,512]{1,0:T(2,128)} %ds_in.1, f32[2,512]{1,0:T(2,128)} %pg_in.1, f32[2,512]{1,0:T(2,128)} %qg_in.1), custom_call_target="tpu_custom_call" | custom-call | tf_op jit(solution)/shard_map/pallas_call | solution.py:428
  143.3 0.7 copy.9

commit v3 on v2

--- a/solution.py
+++ b/solution.py
@@ -12,6 +12,7 @@
 MESH = pl.DeviceIdType.MESH
 STREAMS = 2
 PIECES = 2
+AHEAD = 2
 TAIL_IN_SCATTER = (1, 1, 3, 6)
 TAIL_IN_GATHER = (0, 0, 2, 5)
 LANES = 128
@@ -109,6 +110,8 @@
     def take_up(l, chosen):
         for i in chosen:
             up_copy(l, i).wait()
+            if l == 0 and i + AHEAD < n:
+                up_copy(0, i + AHEAD).start()
             convert(st_up, wu, i, chunk(far_first[i]))
             if l + 1 < layers:
                 up_copy(l + 1, i).start()
@@ -216,11 +219,20 @@
     quarter = rows // m
     others = [(i, k) for i in range(n) for k in range(m) if i or k]
 
-    def share_parts(l, g):
-        for who in range(m):
-            part_s[l, g, who] = acc[g, who * quarter : (who + 1) * quarter, :].astype(bf16)
+    def first_row(who):
+        return (who % PIECES) * sub + who // PIECES * quarter
+
+    def share_parts(l, g, h):
+        c = chunk(far)
+        a = dot(hid[l, g, c, 0, part(h), :], wd[c, :fh, :])
+        a = a + dot(hid[l, g, c, 1, part(h), :], wd[c, fh:, :])
+        a = (a + acc[g, part(h), :]).astype(bf16)
+        for i in range(m // PIECES):
+            part_s[l, g, i * PIECES + h] = a[i * quarter : (i + 1) * quarter, :]
         for k in range(1, m):
-            part_copy(l, g, k).start()
+            @pl.when(lax.rem(cb + k, PIECES) == h)
+            def _():
+                part_copy(l, g, k).start()
 
     def share_sums(l, g):
         v = part_s[l, g, cb].astype(f32)
@@ -253,7 +265,8 @@
                 t = t + ssall[l, g, who, i]
             t = lax.rsqrt(t / (dl * n) + norm_eps)
             inv = jnp.transpose(jnp.broadcast_to(t, (LANES, ssq.shape[0])))[:quarter, :]
-            at = slice(g * rows + who * quarter, g * rows + (who + 1) * quarter)
+            low = first_row(who)
+            at = slice(g * rows + low, g * rows + low + quarter)
             for j in range(dl // LANES):
                 col = slice(j * LANES, (j + 1) * LANES)
                 b = sums[l, g, who, :, col].astype(f32) * ds[l : l + 1, col]
@@ -261,7 +274,7 @@
                 new = (residual_keep * before[at, col].astype(f32) + branch).astype(bf16)
                 out[at, col] = new
                 if l + 1 < layers:
-                    xs[g, who * quarter : (who + 1) * quarter, col] = (
+                    xs[g, low : low + quarter, col] = (
                         new.astype(f32) * pg[l + 1 : l + 2, col]
                     ).astype(bf16)
 
@@ -300,7 +313,7 @@
     ]
     for copy in inputs:
         copy.start()
-    for i in range(n):
+    for i in range(AHEAD):
         up_copy(0, i).start()
     ssq[...] = jnp.zeros_like(ssq)
     for copy in inputs:
@@ -310,18 +323,21 @@
 
     def tail_steps(l, g):
         def end():
-            forward(l, g, far + 1, long_flows)
-            reduce_hidden(l, g, far)
-            share_parts(l, g)
+            for h in range(PIECES):
+                for d, e in long_flows:
+                    ag_copy(l, g, d, e, far, h, arriving=True).wait_recv()
+                share_parts(l, g, h)
 
         def short_end():
             forward(l, g, far, short_flows)
             reduce_hidden(l, g, far - 1)
             reduce_hidden(l, g, 1 - far)
 
-        return [
-            short_end, end, lambda: share_sums(l, g), lambda: renew(l, g),
-        ]
+        def settle():
+            drain_rest(l, g)
+            renew(l, g)
+
+        return [short_end, end, lambda: share_sums(l, g), settle]
 
     def scatter_steps(l, g):
         fresh = l == 0 and g == 0
@@ -337,7 +353,7 @@
         def short(k):
             if fresh:
                 take_up(l, [2 * k - 1, 2 * k])
-                if k == 1:
+                if k == far - 1:
                     for i in range(n):
                         dn_copy(l, i).start()
                 if k == far - 1:
@@ -402,9 +418,6 @@
         pending = tail_steps(l, 1)
     for step in pending:
         step()
-    for l in range(layers):
-        for g in range(STREAMS):
-            drain_rest(l, g)
 
 
 def local(n, m, tokens, up_weight, up_scale, down_weight, down_scale, pre_gain, post_gain):
@@ -412,7 +425,7 @@
     layers, _, fl = up_weight.shape
     fits = (
         n % 2 == 0 and n >= 4 and m >= 2 and t % (STREAMS * PIECES * BF16_ROWS) == 0
-        and t % (STREAMS * m * BF16_ROWS) == 0 and fl % (2 * n * LANES) == 0
+        and m % PIECES == 0 and t % (STREAMS * m * BF16_ROWS) == 0 and fl % (2 * n * LANES) == 0
         and dl % LANES == 0
     )
     if not fits:

time: 144 us -> 141 us (0.979)
  Pallas kernels: 143 us -> 140 us
    pallas_call x1, Pallas kernels: 143 us -> 140 us  [local(): pl.pallas_call(functools.partial(kernel, n, m, layers), out_shape=pltpu.V...]
where the time goes in v3:
time: 141 us
  Pallas kernels  140 us (99%)
    pallas_call x1, Pallas kernels, local(): pl.pallas_call(functools.partial(kernel, n, m, layers), out_shape=pltpu.V...  140 us

profile of v3, /device:TPU:0, one launch (start us, length us, event | category | flops | bytes accessed | tf_op | source)
XLA Modules:
  0.0 141.2 jit_solution(16914191749344190565)
XLA Ops:
  0.0 140.4 %shard_map.73 = bf16[384,512]{1,0:T(8,128)(2,1)S(1)} custom-call(bf16[384,512]{1,0:T(8,128)(2,1)} %tok_in.1, f32[2,512,4096]{2,1,0:T(8,128)} %up.1, f32[2,4096]{1,0:T(2,128)} %us_in.1, f32[2,4096,512]{2,1,0:T(8,128)} %dn.1, f32[2,512]{1,0:T(2,128)} %ds_in.1, f32[2,512]{1,0:T(2,128)} %pg_in.1, f32[2,512]{1,0:T(2,128)} %qg_in.1), custom_call_target="tpu_custom_call" | custom-call | tf_op jit(solution)/shard_map/pallas_call | solution.py:441
  140.4 0.7 copy.9

commit v4 on v3

--- a/solution.py
+++ b/solution.py
@@ -311,15 +311,20 @@
             [(pg_in, pg), (tok_in, tok), (us_in, us), (ds_in, ds), (qg_in, qg)]
         )
     ]
-    for copy in inputs:
+    for copy in inputs[:2]:
         copy.start()
     for i in range(AHEAD):
         up_copy(0, i).start()
+    for copy in inputs[2:]:
+        copy.start()
     ssq[...] = jnp.zeros_like(ssq)
-    for copy in inputs:
+    for copy in inputs[:2]:
         copy.wait()
-    for g in range(STREAMS):
+
+    def scale_in(g):
         xs[g] = (tok[g * rows : (g + 1) * rows, :].astype(f32) * pg[0:1, :]).astype(bf16)
+
+    scale_in(0)
 
     def tail_steps(l, g):
         def end():
@@ -349,6 +354,11 @@
             if fresh:
                 pl.semaphore_wait(barrier, m + 1)
             scatter(l, g, 0, long_flows)
+            if fresh:
+                for later in range(1, STREAMS):
+                    scale_in(later)
+                for copy in inputs[2:]:
+                    copy.wait()
 
         def short(k):
             if fresh:

time: 141 us -> 141 us (level)
  no operation moved by 1% of the time
where the time goes in v4:
time: 141 us
  Pallas kernels  140 us (99%)
    pallas_call x1, Pallas kernels, local(): pl.pallas_call(functools.partial(kernel, n, m, layers), out_shape=pltpu.V...  140 us

profile of v4, /device:TPU:0, one launch (start us, length us, event | category | flops | bytes accessed | tf_op | source)
XLA Modules:
  0.0 141.2 jit_solution(3605075475170309094)
XLA Ops:
  0.0 140.4 %shard_map.73 = bf16[384,512]{1,0:T(8,128)(2,1)S(1)} custom-call(bf16[384,512]{1,0:T(8,128)(2,1)} %tok_in.1, f32[2,512,4096]{2,1,0:T(8,128)} %up.1, f32[2,4096]{1,0:T(2,128)} %us_in.1, f32[2,4096,512]{2,1,0:T(8,128)} %dn.1, f32[2,512]{1,0:T(2,128)} %ds_in.1, f32[2,512]{1,0:T(2,128)} %pg_in.1, f32[2,512]{1,0:T(2,128)} %qg_in.1), custom_call_target="tpu_custom_call" | custom-call | tf_op jit(solution)/shard_map/pallas_call | solution.py:451
  140.4 0.7 copy.9
